TPU v7x, 32 devices: a whole 2x2x4 slice. The times are simulated.
32 devices in a mesh: fs: 16 (over z, y, core), tp: 2 (over x).
Axes of the slice: x: 2, y: 2, z: 4, core: 2. Of those that a mesh axis runs over, the one named last changes fastest.
Arguments:
- inputs: bfloat16 [16384, 3072], P('fs'), may hold values from -6 to 6
- query_cot: bfloat16 [16384, 768], P('fs', 'tp'), may hold values from -0.046875 to 0.046875
- value_cot: bfloat16 [16384, 1536], P('fs', 'tp'), may hold values from -0.046875 to 0.046875
- query_factor: bfloat16 [3072, 192], P('fs'), may hold values from -0.109375 to 0.109375
- value_factor: bfloat16 [3072, 192], P('fs'), may hold values from -0.109375 to 0.109375
- query_weight: float32 [3072, 768], P('fs', 'tp'), may hold values from -0.109375 to 0.109375
- value_weight: float32 [3072, 1536], P('fs', 'tp'), may hold values from -0.109375 to 0.109375
- query_first: float32 [192, 768], P('fs', 'tp'), may hold values from -1.6 to 1.6
- query_second: float32 [192, 768], P('fs', 'tp'), may hold values from 0.002 to 0.05
- value_first: float32 [192, 1536], P('fs', 'tp'), may hold values from -1.6 to 1.6
- value_second: float32 [192, 1536], P('fs', 'tp'), may hold values from 0.002 to 0.05
Outputs:
- step_q: float32 [3072, 768], P('fs', 'tp')
- step_v: float32 [3072, 1536], P('fs', 'tp')
- new_q: float32 [3072, 768], P('fs', 'tp')
- new_v: float32 [3072, 1536], P('fs', 'tp')
- first_q: float32 [192, 768], P('fs', 'tp')
- second_q: float32 [192, 768], P('fs', 'tp')
- first_v: float32 [192, 1536], P('fs', 'tp')
- second_v: float32 [192, 1536], P('fs', 'tp')
- copy_q: bfloat16 [3072, 768], P(None, 'tp')
- copy_v: bfloat16 [3072, 1536], P(None, 'tp')
All inputs are finite; a program needn't handle non-finite values.
Results may differ from a plain program's by a relative error of at most 0.0041.
Values may be sent and summed in bfloat16 or wider, within the bound.
A program may use at most 64 MiB of HBM per device.

v0:
```python
import jax
import jax.numpy as jnp
from jax import lax
from jax.sharding import PartitionSpec as P

first_decay = 0.9
second_decay = 0.99
small_eps = 1e-08
learn_rate = 0.01


def moments(old_first, old_second, gradient):
    first = first_decay * old_first + (1.0 - first_decay) * gradient
    second = second_decay * old_second + (1.0 - second_decay) * gradient * gradient
    unit = first / (jnp.sqrt(second) + small_eps)
    return (first, second, unit)


def on_device(
    inputs,
    query_cot,
    value_cot,
    query_factor,
    value_factor,
    query_weight,
    value_weight,
    query_first,
    query_second,
    value_first,
    value_second,
):
    rank_cols = query_factor.shape[1]
    q_cols = query_cot.shape[1]
    v_cols = value_cot.shape[1]
    own_rows = query_first.shape[0]
    entries = rank_cols * (q_cols + v_cols) * lax.axis_size("tp")
    full_qf, full_vf = (
        lax.all_gather(query_factor, "fs", axis=0, tiled=True),
        lax.all_gather(value_factor, "fs", axis=0, tiled=True),
    )
    sum_q = jnp.dot(inputs, full_qf, preferred_element_type=jnp.float32)
    sum_v = jnp.dot(inputs, full_vf, preferred_element_type=jnp.float32)
    proj_q = sum_q.astype(jnp.bfloat16)
    proj_v = sum_v.astype(jnp.bfloat16)
    term_q = lax.dot_general(
        proj_q, query_cot, (((0,), (0,)), ((), ())), preferred_element_type=jnp.float32
    )
    term_v = lax.dot_general(
        proj_v, value_cot, (((0,), (0,)), ((), ())), preferred_element_type=jnp.float32
    )
    full_sums = lax.psum(jnp.concatenate([term_q, term_v], axis=1), "fs")
    stacked = (
        lax.all_gather(query_first, "fs", axis=0, tiled=True),
        lax.all_gather(query_second, "fs", axis=0, tiled=True),
        lax.all_gather(value_first, "fs", axis=0, tiled=True),
        lax.all_gather(value_second, "fs", axis=0, tiled=True),
    )
    all_first_q, all_second_q, unit_q = moments(stacked[0], stacked[1], full_sums[:, :q_cols])
    all_first_v, all_second_v, unit_v = moments(stacked[2], stacked[3], full_sums[:, q_cols:])
    norm_total = lax.psum(jnp.sum(unit_q * unit_q) + jnp.sum(unit_v * unit_v), "tp")
    step_scale = lax.rsqrt(norm_total / entries + 1e-06)
    whole_q = (step_scale * unit_q).astype(jnp.bfloat16)
    whole_v = (step_scale * unit_v).astype(jnp.bfloat16)
    row_begin = lax.axis_index("fs") * own_rows
    first_q = lax.dynamic_slice_in_dim(all_first_q, row_begin, own_rows, 0)
    second_q = lax.dynamic_slice_in_dim(all_second_q, row_begin, own_rows, 0)
    first_v = lax.dynamic_slice_in_dim(all_first_v, row_begin, own_rows, 0)
    second_v = lax.dynamic_slice_in_dim(all_second_v, row_begin, own_rows, 0)
    step_q = jnp.dot(query_factor, whole_q, preferred_element_type=jnp.float32)
    step_v = jnp.dot(value_factor, whole_v, preferred_element_type=jnp.float32)
    new_q = query_weight - learn_rate * step_q
    new_v = value_weight - learn_rate * step_v
    copy_q, copy_v = (
        lax.all_gather(new_q.astype(jnp.bfloat16), "fs", axis=0, tiled=True),
        lax.all_gather(new_v.astype(jnp.bfloat16), "fs", axis=0, tiled=True),
    )
    return (step_q, step_v, new_q, new_v, first_q, second_q, first_v, second_v, copy_q, copy_v)


def solution(mesh):
    in_specs = (
        P("fs", None),
        P("fs", "tp"),
        P("fs", "tp"),
        P("fs", None),
        P("fs", None),
        P("fs", "tp"),
        P("fs", "tp"),
        P("fs", "tp"),
        P("fs", "tp"),
        P("fs", "tp"),
        P("fs", "tp"),
    )
    out_specs = (
        P("fs", "tp"),
        P("fs", "tp"),
        P("fs", "tp"),
        P("fs", "tp"),
        P("fs", "tp"),
        P("fs", "tp"),
        P("fs", "tp"),
        P("fs", "tp"),
        P(None, "tp"),
        P(None, "tp"),
    )
    return jax.shard_map(
        on_device, mesh=mesh, in_specs=in_specs, out_specs=out_specs, check_vma=False
    )
```

profile of v0, /device:TPU:0, one launch (start us, length us, event | category | flops | bytes accessed | tf_op | source)
XLA Modules:
  0.0 321.6 jit_solution(11538157095303594677)
XLA Ops:
  7.2 0.7 all-gather.11.cloned.1.call-update
  8.0 0.7 all-gather.9.cloned.1.call-update
  8.7 24.6 %all-gather = f32[16,12,384]{2,1,0:T(8,128)S(1)} all-gather(f32[1,12,384]{2,1,0:T(8,128)} %bitcast.18), channel_id=1, replica_groups=mesh['fs'=16,'tp'=2] {'fs'}, dimensions={0}, use_global_device_ids=true | all-gather | bytes 313344 | tf_op jit(solution)/shard_map/all_gather | solution.py:53
  33.4 21.9 %all-gather.2 = f32[16,12,768]{2,1,0:T(8,128)S(1)} all-gather(f32[1,12,768]{2,1,0:T(8,128)} %bitcast.16), channel_id=1, replica_groups=mesh['fs'=16,'tp'=2] {'fs'}, dimensions={0}, use_global_device_ids=true | all-gather | bytes 626688 | tf_op jit(solution)/shard_map/all_gather | solution.py:55
  55.3 0.1 broadcast_multiply_fusion.1
  55.4 21.1 %all-gather.3 = f32[16,12,768]{2,1,0:T(8,128)S(1)} all-gather(f32[1,12,768]{2,1,0:T(8,128)S(1)} %bitcast.17), channel_id=1, replica_groups=mesh['fs'=16,'tp'=2] {'fs'}, dimensions={0}, use_global_device_ids=true | all-gather | bytes 626688 | tf_op jit(solution)/shard_map/all_gather | solution.py:56
  76.5 0.1 broadcast_multiply_fusion
  76.6 6.6 %fusion.1 = f32[192,768]{1,0:T(8,128)} fusion(bf16[1024,768]{1,0:T(8,128)(2,1)S(1)} %copy-done, bf16[1024,3072]{1,0:T(8,128)(2,1)} %param.11, bf16[3072,192]{1,0:T(8,128)(2,1)} %all-gather.11.cloned.1.call-done), kind=kOutput, calls=%fused_computation.5 | convolution fusion | flops 1510146048 | bytes 9633792 | tf_op jit(solution)/shard_map/dot_general | solution.py:48
  83.3 15.3 %all-gather.9.cloned.1.call-done = bf16[3072,192]{1,0:T(8,128)(2,1)} async-done(((bf16[192,192]{1,0:T(8,128)(2,1)}), bf16[3072,192]{1,0:T(8,128)(2,1)}) %all-gather.9.cloned.1.call-update) | async-done | bytes 1179664 | tf_op jit(solution)/shard_map/all_gather | solution.py:38
  98.5 6.5 %fusion = f32[192,384]{1,0:T(8,128)} fusion(bf16[1024,384]{1,0:T(8,128)(2,1)} %param.12, bf16[1024,3072]{1,0:T(8,128)(2,1)} %param.11, bf16[3072,192]{1,0:T(8,128)(2,1)} %all-gather.9.cloned.1.call-done), kind=kOutput, calls=%fused_computation.4 | convolution fusion | flops 1359151104 | bytes 8552448 | tf_op jit(solution)/shard_map/dot_general | solution.py:45
  105.0 2.1 pad_maximum_fusion
  107.2 0.0 all-gather.13.cloned.1.call-start
  107.2 0.8 broadcast_multiply_fusion.3
  108.0 0.9 reshape.33
  108.9 0.9 reshape.35
  109.8 0.2 copy-done.3
  110.0 0.7 reshape.29
  110.7 20.7 %all-gather.1 = f32[16,12,384]{2,1,0:T(8,128)S(1)} all-gather(f32[1,12,384]{2,1,0:T(8,128)S(1)} %bitcast.19), channel_id=1, replica_groups=mesh['fs'=16,'tp'=2] {'fs'}, dimensions={0}, use_global_device_ids=true | all-gather | bytes 313344 | tf_op jit(solution)/shard_map/all_gather | solution.py:54
  131.4 0.7 reshape.31
  132.2 67.6 %all-reduce.2.cloned.1.call-done = f32[192,1152]{1,0:T(8,128)} async-done(((f32[192,1152]{1,0:T(8,128)}), f32[192,1152]{1,0:T(8,128)}) %all-reduce.2.cloned.1.call-update) | async-done | bytes 884752 | tf_op jit(solution)/shard_map/psum | solution.py:51
  199.7 2.2 multiply_reduce_fusion
  202.0 1.8 multiply_reduce_fusion.1
  205.1 5.4 %psum.15 = f32[]{:T(128)} all-reduce(f32[]{:T(128)S(6)} %add.48), channel_id=1, replica_groups=mesh['fs'=16,'tp'=2] {'tp'}, use_global_device_ids=true, to_apply=%region_3.0 | all-reduce | flops 1 | bytes 8 | tf_op jit(solution)/shard_map/psum | solution.py:60
  211.2 2.1 fusion.7
  213.3 0.0 all-gather.15.cloned.1.call-start
  213.4 2.6 fusion.6
  216.0 0.6 constant_dynamic-slice_fusion.2
  216.7 0.6 constant_dynamic-slice_fusion
  217.3 37.5 %all-gather.13.cloned.1.call-done = bf16[3072,384]{1,0:T(8,128)(2,1)} async-done(((bf16[192,384]{1,0:T(8,128)(2,1)}), bf16[3072,384]{1,0:T(8,128)(2,1)}) %all-gather.13.cloned.1.call-update) | async-done | bytes 2359312 | tf_op jit(solution)/shard_map/all_gather | solution.py:74
  254.8 54.6 %all-gather.15.cloned.1.call-done = bf16[3072,768]{1,0:T(8,128)(2,1)} async-done(((bf16[192,768]{1,0:T(8,128)(2,1)}), bf16[3072,768]{1,0:T(8,128)(2,1)}) %all-gather.15.cloned.1.call-update) | async-done | bytes 4718608 | tf_op jit(solution)/shard_map/all_gather | solution.py:75
  309.4 3.5 %copy.24 = bf16[3072,384]{1,0:T(8,128)(2,1)} copy(bf16[3072,384]{1,0:T(8,128)(2,1)} %all-gather.13.cloned.1.call-done) | data formatting | bytes 4718592
  312.8 2.2 copy.25
  (27 shorter events, 0.3 us)
Async XLA Ops:
  7.2 69.5 %copy-start = (bf16[1024,768]{1,0:T(8,128)(2,1)S(1)}, bf16[1024,768]{1,0:T(8,128)(2,1)}, u32[]{:S(2)}) copy-start(bf16[1024,768]{1,0:T(8,128)(2,1)} %param.13) | copy-start | bytes 4718596
  7.2 48.2 %copy-start.8 = (f32[12,768]{1,0:T(8,128)S(1)}, f32[12,768]{1,0:T(8,128)}, u32[]{:S(2)}) copy-start(f32[12,768]{1,0:T(8,128)} %param.21) | copy-start | bytes 110596
  7.2 69.4 %all-gather.11.cloned.1.call-start = ((), (), s32[]{:S(2)}) async-start(), calls=%async_computation.1 | async-start | bytes 1671168 | tf_op jit(solution)/shard_map/all_gather | solution.py:39
  7.9 90.6 %all-gather.9.cloned.1.call-start = ((), (), s32[]{:S(2)}) async-start(), calls=%async_computation | async-start | bytes 1671168 | tf_op jit(solution)/shard_map/all_gather | solution.py:38
  8.7 191.0 %all-reduce.2.cloned.1.call-start = ((), (), s32[]{:S(2)}) async-start(), calls=%async_computation.2 | async-start | bytes 1769472 | tf_op jit(solution)/shard_map/psum | solution.py:51
  107.2 147.6 %all-gather.13.cloned.1.call-start = ((), (), s32[]{:S(2)}) async-start(), calls=%async_computation.3 | async-start | bytes 2506752 | tf_op jit(solution)/shard_map/all_gather | solution.py:74
  108.9 1.1 copy-start.3
  108.9 1.8 copy-start.9
  110.0 89.8 %copy-start.2 = (f32[192,768]{1,0:T(8,128)S(1)}, f32[192,768]{1,0:T(8,128)}, u32[]{:S(2)}) copy-start(f32[192,768]{1,0:T(8,128)} %reshape.33) | copy-start | bytes 1769476
  132.2 79.0 %copy-start.7 = (bf16[192,192]{1,0:T(8,128)(2,1)S(1)}, bf16[192,192]{1,0:T(8,128)(2,1)}, u32[]{:S(2)}) copy-start(bf16[192,192]{1,0:T(8,128)(2,1)} %param.14) | copy-start | bytes 221188
  199.7 2.2 copy-start.4
  199.7 2.2 copy-start.5
  202.0 11.4 %copy-start.6 = (bf16[192,192]{1,0:T(8,128)(2,1)S(1)}, bf16[192,192]{1,0:T(8,128)(2,1)}, u32[]{:S(2)}) copy-start(bf16[192,192]{1,0:T(8,128)(2,1)} %param.15) | copy-start | bytes 221188
  213.3 96.0 %all-gather.15.cloned.1.call-start = ((), (), s32[]{:S(2)}) async-start(), calls=%async_computation.4 | async-start | bytes 5013504 | tf_op jit(solution)/shard_map/all_gather | solution.py:75
  309.4 3.5 %copy-start.1 = (bf16[3072,768]{1,0:T(8,128)(2,1)S(1)}, bf16[3072,768]{1,0:T(8,128)(2,1)}, u32[]{:S(2)}) copy-start(bf16[3072,768]{1,0:T(8,128)(2,1)} %all-gather.15.cloned.1.call-done) | copy-start | bytes 14155780
Sparse Core Ops, SparseCore 0:
  10.3 43.8 all-gather.10
  56.4 42.0 all-gather.8
  107.3 92.3 all-reduce.1
  213.5 41.3 all-gather.12
  257.5 51.8 all-gather.14
where the time goes:
time: 322 us
  waiting for transfers between devices  176 us (55%)
  blocking collectives  93.8 us (29%)
  matrix products  17.9 us (6%)
  between operations  15.9 us (5%)
  local copies, waits for them, and re-layouts  10.4 us (3%)
  other arithmetic  7.08 us (2%)
    psum x1, waiting for transfers between devices, on_device(): full_sums = lax.psum(jnp.concatenate([term_q, term_v], axis=1), 'fs')  67.6 us
    all_gather x1, waiting for transfers between devices, on_device(): lax.all_gather(new_v.astype(jnp.bfloat16), 'fs', axis=0, tiled=True)  54.6 us
    all_gather x1, waiting for transfers between devices, on_device(): lax.all_gather(new_q.astype(jnp.bfloat16), 'fs', axis=0, tiled=True)  37.5 us
    all_gather x1, blocking collectives, on_device(): lax.all_gather(query_first, 'fs', axis=0, tiled=True)  24.6 us
    all_gather x1, blocking collectives, on_device(): lax.all_gather(value_first, 'fs', axis=0, tiled=True)  21.9 us
    all_gather x1, blocking collectives, on_device(): lax.all_gather(value_second, 'fs', axis=0, tiled=True)  21.1 us
    all_gather x1, blocking collectives, on_device(): lax.all_gather(query_second, 'fs', axis=0, tiled=True)  20.7 us
    all_gather x1, waiting for transfers between devices, on_device(): lax.all_gather(query_factor, 'fs', axis=0, tiled=True)  15.3 us
  transfers between devices with their start and end apart: 5, of which 4 were waited for; matrix products, arithmetic and copies ran while one was open for 5% of the time, Pallas kernels for 0%

commit v1 on v0

--- a/solution.py
+++ b/solution.py
@@ -2,6 +2,7 @@
 import jax.numpy as jnp
 from jax import lax
 from jax.sharding import PartitionSpec as P
+from jax.lax import all_gather
 
 first_decay = 0.9
 second_decay = 0.99
@@ -48,7 +49,8 @@
     term_v = lax.dot_general(
         proj_v, value_cot, (((0,), (0,)), ((), ())), preferred_element_type=jnp.float32
     )
-    full_sums = lax.psum(jnp.concatenate([term_q, term_v], axis=1), "fs")
+    row_data = jnp.concatenate([term_q, term_v], axis=1)
+    full_sums = all_gather(row_data, "fs").sum(axis=0)
     stacked = (
         lax.all_gather(query_first, "fs", axis=0, tiled=True),
         lax.all_gather(query_second, "fs", axis=0, tiled=True),

time: 322 us -> 350 us (1.087)
  waiting for transfers between devices: 176 us -> 195 us
  other arithmetic: 7.08 us -> 11.4 us
  blocking collectives: 93.8 us -> 97.9 us
    psum x1 -> x0, waiting for transfers between devices: 67.6 us -> none  [on_device(): full_sums = lax.psum(jnp.concatenate([term_q, term_v], axis=1), 'fs')]
    all_gather x1, waiting for transfers between devices: 0.02 us -> 43.9 us  [on_device(): lax.all_gather(value_factor, 'fs', axis=0, tiled=True)]
    all_gather x0 -> x1, waiting for transfers between devices: none -> 25.8 us  [on_device(): full_sums = all_gather(row_data, 'fs').sum(axis=0)]
    all_gather x1, waiting for transfers between devices: 15.3 us -> 34.8 us  [on_device(): lax.all_gather(query_factor, 'fs', axis=0, tiled=True)]
    reduce_sum x0 -> x1, other arithmetic: none -> 5.76 us  [on_device(): full_sums = all_gather(row_data, 'fs').sum(axis=0)]
  transfers between devices with their start and end apart: 5 -> 5, of which waited for: 4 -> 5; matrix products, arithmetic and copies ran while one was open for 5% -> 4% of each run, Pallas kernels for 0% -> 0%
where the time goes in v1:
time: 350 us; the launch traced here: 349 us
  waiting for transfers between devices  195 us (56%)
  blocking collectives  97.9 us (28%)
  matrix products  16.4 us (5%)
  between operations  15.9 us (5%)
  local copies, waits for them, and re-layouts  11.9 us (3%)
  other arithmetic  11.4 us (3%)
    all_gather x1, waiting for transfers between devices, on_device(): lax.all_gather(new_v.astype(jnp.bfloat16), 'fs', axis=0, tiled=True)  54 us
    all_gather x1, waiting for transfers between devices, on_device(): lax.all_gather(value_factor, 'fs', axis=0, tiled=True)  43.9 us
    all_gather x1, waiting for transfers between devices, on_device(): lax.all_gather(new_q.astype(jnp.bfloat16), 'fs', axis=0, tiled=True)  35.3 us
    all_gather x1, waiting for transfers between devices, on_device(): lax.all_gather(query_factor, 'fs', axis=0, tiled=True)  34.8 us
    all_gather x1, waiting for transfers between devices, on_device(): full_sums = all_gather(row_data, 'fs').sum(axis=0)  25.8 us
    all_gather x1, blocking collectives, on_device(): lax.all_gather(value_second, 'fs', axis=0, tiled=True)  24.2 us
    all_gather x1, blocking collectives, on_device(): lax.all_gather(value_first, 'fs', axis=0, tiled=True)  23.7 us
    all_gather x1, blocking collectives, on_device(): lax.all_gather(query_second, 'fs', axis=0, tiled=True)  22.7 us
  transfers between devices with their start and end apart: 5, of which 5 were waited for; matrix products, arithmetic and copies ran while one was open for 4% of the time, Pallas kernels for 0%

profile of v1, /device:TPU:0, one launch (start us, length us, event | category | flops | bytes accessed | tf_op | source)
XLA Modules:
  0.0 349.1 jit_solution(1508407775567226340)
XLA Ops:
  7.2 0.7 all-gather.13.cloned.1.call-update
  8.0 0.7 all-gather.11.cloned.1.call-update
  8.7 43.9 %all-gather.13.cloned.1.call-done = bf16[3072,192]{1,0:T(8,128)(2,1)} async-done(((bf16[192,192]{1,0:T(8,128)(2,1)}), bf16[3072,192]{1,0:T(8,128)(2,1)}) %all-gather.13.cloned.1.call-update) | async-done | bytes 1179664 | tf_op jit(solution)/shard_map/all_gather | solution.py:40
  52.6 5.8 %fusion.1 = f32[192,768]{1,0:T(8,128)S(1)} fusion(bf16[1024,768]{1,0:T(8,128)(2,1)S(1)} %copy-done, bf16[1024,3072]{1,0:T(8,128)(2,1)} %param.11, bf16[3072,192]{1,0:T(8,128)(2,1)} %all-gather.13.cloned.1.call-done), kind=kOutput, calls=%fused_computation.5 | convolution fusion | flops 1510146048 | bytes 9633792 | tf_op jit(solution)/shard_map/dot_general | solution.py:49
  58.4 34.8 %all-gather.11.cloned.1.call-done = bf16[3072,192]{1,0:T(8,128)(2,1)} async-done(((bf16[192,192]{1,0:T(8,128)(2,1)}), bf16[3072,192]{1,0:T(8,128)(2,1)}) %all-gather.11.cloned.1.call-update) | async-done | bytes 1179664 | tf_op jit(solution)/shard_map/all_gather | solution.py:39
  93.3 5.6 %fusion = f32[192,384]{1,0:T(8,128)S(1)} fusion(bf16[1024,384]{1,0:T(8,128)(2,1)S(1)} %copy-done.10, bf16[1024,3072]{1,0:T(8,128)(2,1)} %param.11, bf16[3072,192]{1,0:T(8,128)(2,1)} %all-gather.11.cloned.1.call-done), kind=kOutput, calls=%fused_computation.4 | convolution fusion | flops 1359151104 | bytes 8552448 | tf_op jit(solution)/shard_map/dot_general | solution.py:46
  98.9 1.0 pad_maximum_fusion
  99.9 0.0 all-gather.15.cloned.1.call-start
  100.0 23.7 %all-gather.3 = f32[16,12,768]{2,1,0:T(8,128)S(1)} all-gather(f32[1,12,768]{2,1,0:T(8,128)S(1)} %bitcast.18), channel_id=1, replica_groups=mesh['fs'=16,'tp'=2] {'fs'}, dimensions={0}, use_global_device_ids=true | all-gather | bytes 626688 | tf_op jit(solution)/shard_map/all_gather | solution.py:57
  123.7 0.1 broadcast_multiply_fusion.1
  123.8 0.9 reshape.34
  124.7 24.2 %all-gather.4 = f32[16,12,768]{2,1,0:T(8,128)S(1)} all-gather(f32[1,12,768]{2,1,0:T(8,128)S(1)} %bitcast.19), channel_id=1, replica_groups=mesh['fs'=16,'tp'=2] {'fs'}, dimensions={0}, use_global_device_ids=true | all-gather | bytes 626688 | tf_op jit(solution)/shard_map/all_gather | solution.py:58
  148.9 0.1 broadcast_multiply_fusion
  149.0 0.9 reshape.36
  149.9 21.8 %all-gather.1 = f32[16,12,384]{2,1,0:T(8,128)S(1)} all-gather(f32[1,12,384]{2,1,0:T(8,128)S(1)} %bitcast.20), channel_id=1, replica_groups=mesh['fs'=16,'tp'=2] {'fs'}, dimensions={0}, use_global_device_ids=true | all-gather | bytes 313344 | tf_op jit(solution)/shard_map/all_gather | solution.py:55
  171.7 0.7 reshape.30
  172.4 22.7 %all-gather.2 = f32[16,12,384]{2,1,0:T(8,128)S(1)} all-gather(f32[1,12,384]{2,1,0:T(8,128)S(1)} %bitcast.21), channel_id=1, replica_groups=mesh['fs'=16,'tp'=2] {'fs'}, dimensions={0}, use_global_device_ids=true | all-gather | bytes 313344 | tf_op jit(solution)/shard_map/all_gather | solution.py:56
  195.2 0.7 reshape.32
  196.0 25.8 %all-gather.19.cloned.1.call-done = f32[3072,1152]{1,0:T(8,128)} async-done(((f32[192,1152]{1,0:T(8,128)}), f32[3072,1152]{1,0:T(8,128)}) %all-gather.19.cloned.1.call-update) | async-done | bytes 14155792 | tf_op jit(solution)/shard_map/all_gather | solution.py:53
  221.8 5.8 %reduce_sum.27 = f32[192,1152]{1,0:T(8,128)S(1)} reduce(f32[16,192,1152]{2,1,0:T(8,128)} %bitcast.17, f32[]{:T(128)} %constant.14.clone.1), dimensions={0}, to_apply=%region_0.0 | reduce | flops 3317760 | bytes 15040516 | tf_op jit(solution)/shard_map/reduce_sum | solution.py:53
  227.6 3.0 multiply_reduce_fusion
  230.6 1.5 multiply_reduce_fusion.1
  233.4 5.4 %psum.7 = f32[]{:T(128)} all-reduce(f32[]{:T(128)S(6)} %add.46), channel_id=1, replica_groups=mesh['fs'=16,'tp'=2] {'tp'}, use_global_device_ids=true, to_apply=%region_3.0 | all-reduce | flops 1 | bytes 8 | tf_op jit(solution)/shard_map/psum | solution.py:62
  239.5 2.2 fusion.7
  241.7 0.0 all-gather.17.cloned.1.call-start
  241.8 2.8 fusion.6
  244.6 1.4 constant_dynamic-slice_fusion.2
  246.0 1.5 constant_dynamic-slice_fusion
  247.5 35.3 %all-gather.15.cloned.1.call-done = bf16[3072,384]{1,0:T(8,128)(2,1)} async-done(((bf16[192,384]{1,0:T(8,128)(2,1)}), bf16[3072,384]{1,0:T(8,128)(2,1)}) %all-gather.15.cloned.1.call-update) | async-done | bytes 2359312 | tf_op jit(solution)/shard_map/all_gather | solution.py:76
  282.9 54.0 %all-gather.17.cloned.1.call-done = bf16[3072,768]{1,0:T(8,128)(2,1)} async-done(((bf16[192,768]{1,0:T(8,128)(2,1)}), bf16[3072,768]{1,0:T(8,128)(2,1)}) %all-gather.17.cloned.1.call-update) | async-done | bytes 4718608 | tf_op jit(solution)/shard_map/all_gather | solution.py:77
  336.9 3.5 copy.23
  340.3 2.2 copy.24
  (30 shorter events, 0.3 us)
Async XLA Ops:
  7.2 45.5 %copy-start = (bf16[1024,768]{1,0:T(8,128)(2,1)S(1)}, bf16[1024,768]{1,0:T(8,128)(2,1)}, u32[]{:S(2)}) copy-start(bf16[1024,768]{1,0:T(8,128)(2,1)} %param.13) | copy-start | bytes 4718596
  7.2 45.4 %all-gather.13.cloned.1.call-start = ((), (), s32[]{:S(2)}) async-start(), calls=%async_computation.1 | async-start | bytes 1671168 | tf_op jit(solution)/shard_map/all_gather | solution.py:40
  7.9 85.3 %all-gather.11.cloned.1.call-start = ((), (), s32[]{:S(2)}) async-start(), calls=%async_computation | async-start | bytes 1671168 | tf_op jit(solution)/shard_map/all_gather | solution.py:39
  8.7 84.6 %copy-start.10 = (bf16[1024,384]{1,0:T(8,128)(2,1)S(1)}, bf16[1024,384]{1,0:T(8,128)(2,1)}, u32[]{:S(2)}) copy-start(bf16[1024,384]{1,0:T(8,128)(2,1)} %param.12) | copy-start | bytes 2359300
  8.7 213.1 %all-gather.19.cloned.1.call-start = ((), (), s32[]{:S(2)}) async-start(), calls=%async_computation.4 | async-start | bytes 15040512 | tf_op jit(solution)/shard_map/all_gather | solution.py:53
  98.9 1.1 copy-start.6
  99.9 24.8 %copy-start.7 = (f32[12,768]{1,0:T(8,128)S(1)}, f32[12,768]{1,0:T(8,128)}, u32[]{:S(2)}) copy-start(f32[12,768]{1,0:T(8,128)} %param.21) | copy-start | bytes 110596
  99.9 183.0 %all-gather.15.cloned.1.call-start = ((), (), s32[]{:S(2)}) async-start(), calls=%async_computation.2 | async-start | bytes 2506752 | tf_op jit(solution)/shard_map/all_gather | solution.py:76
  123.8 26.1 %copy-start.8 = (f32[12,384]{1,0:T(8,128)S(1)}, f32[12,384]{1,0:T(8,128)}, u32[]{:S(2)}) copy-start(f32[12,384]{1,0:T(8,128)} %param.18) | copy-start | bytes 55300
  148.9 23.5 %copy-start.9 = (f32[12,384]{1,0:T(8,128)S(1)}, f32[12,384]{1,0:T(8,128)}, u32[]{:S(2)}) copy-start(f32[12,384]{1,0:T(8,128)} %param.19) | copy-start | bytes 55300
  227.5 3.1 copy-start.2
  227.6 3.1 copy-start.3
  227.6 11.9 %copy-start.5 = (bf16[192,192]{1,0:T(8,128)(2,1)S(1)}, bf16[192,192]{1,0:T(8,128)(2,1)}, u32[]{:S(2)}) copy-start(bf16[192,192]{1,0:T(8,128)(2,1)} %param.14) | copy-start | bytes 221188
  230.6 11.2 %copy-start.4 = (bf16[192,192]{1,0:T(8,128)(2,1)S(1)}, bf16[192,192]{1,0:T(8,128)(2,1)}, u32[]{:S(2)}) copy-start(bf16[192,192]{1,0:T(8,128)(2,1)} %param.15) | copy-start | bytes 221188
  241.7 95.1 %all-gather.17.cloned.1.call-start = ((), (), s32[]{:S(2)}) async-start(), calls=%async_computation.3 | async-start | bytes 5013504 | tf_op jit(solution)/shard_map/all_gather | solution.py:77
  336.9 3.5 copy-start.1
Sparse Core Ops, SparseCore 0:
  10.3 42.3 all-gather.12
  54.9 38.2 all-gather.10
  100.0 121.6 all-gather.18
  241.9 40.9 all-gather.14
  285.0 51.8 all-gather.16
